TPU v7x, 512 devices: a whole 4x8x8 slice. The times are simulated.
512 devices in a mesh: sp: 32 (over z, x), tp: 16 (over y, core).
Axes of the slice: x: 4, y: 8, z: 8, core: 2. Of those that a mesh axis runs over, the one named last changes fastest.
Arguments:
- residual: bfloat16 [8192, 2048], P('sp', 'tp'), may hold values from -6 to 6
- queries: bfloat16 [8192, 1024], P('sp', 'tp'), may hold values from -5.5 to 5.5
- keys: bfloat16 [8192, 128], P('sp'), may hold values from -5.5 to 5.5
- values: bfloat16 [8192, 128], P('sp'), may hold values from -6 to 6
- documents: int32 [8192], P('sp'), may hold values from 0 to 15, never falling along the last dimension, each value on 1 to 1024 neighbouring positions
- sinks: float32 [16], P('tp'), may hold values from 1 to 6
- head_gain: float32 [1024], replicated, may hold values from 0.1 to 1.9
- out_weight: bfloat16 [1024, 2048], P(None, 'tp'), may hold values from -0.1875 to 0.1875
- norm_gain: float32 [2048], P('tp'), may hold values from 0.1 to 1.9
- norm_shift: float32 [2048], P('tp'), may hold values from -3 to 3
- routes: int32 [8192, 2], P('sp'), may hold values from 0 to 31, all different within a row; in each aligned block of 256 rows (0 to 255, 256 to 511, ...) at most 24 rows name the same one
- route_logits: float32 [8192, 2], P('sp'), may hold values from -150 to 150
- gate_weight: bfloat16 [32, 2048, 6144], P('sp', None, 'tp'), may hold values from -0.125 to 0.125
- up_weight: bfloat16 [32, 2048, 6144], P('sp', None, 'tp'), may hold values from -0.125 to 0.125
- down_weight: bfloat16 [32, 6144, 2048], P('sp', 'tp'), may hold values from -0.15625 to 0.15625
- final_gain: float32 [2048], P('tp'), may hold values from 0.1 to 1.9
- final_shift: float32 [2048], P('tp'), may hold values from -3 to 3
Outputs:
- layer_out: bfloat16 [8192, 2048], P('sp', 'tp')
Inputs may be any that keep to these rules, and one draw needn't show every extreme that they name: `documents`: document numbers never fall along the sequence; each document has at least one position and at most 1024, and some document has exactly 1024. `routes`: each row names 2 different experts. In each aligned block of 256 rows (the rows of one index of sp) no expert is named by more than 24 rows, a bound that some block reaches.
All inputs are finite; a program needn't handle non-finite values.
Results may differ from a plain program's by a relative error of at most 0.014.
Values may be sent and summed in bfloat16 or wider, within the bound.
A program may use at most 128 MiB of HBM per device.

v0:
```python
import jax
import jax.numpy as jnp
from jax import lax
from jax.sharding import PartitionSpec as P

D = 2048
QUERY_HEADS = 16
KEY_VALUE_HEADS = 2
HEAD_SIZE = 64
WINDOW_SIZE = 128
TOP = 2
DEEP_ALPHA = 8.0**0.25
NORM_EPS = 1e-05


def sent_to_all(value, axis):
    length = lax.axis_size(axis)
    return lax.all_to_all(
        jnp.broadcast_to(value[None], (length, *value.shape)), axis, 0, 0, tiled=True
    )


def over_copies(value, axis):
    return sent_to_all(value, axis).sum(axis=0)


def in_one(arrays, axis):
    line, at, gathered = (jnp.concatenate([a.reshape(-1) for a in arrays]), 0, [])
    total = over_copies(line, axis)
    for a in arrays:
        gathered.append(total[at : at + a.size].reshape(a.shape))
        at += a.size
    return tuple(gathered)


def shifted(block, axis, distance):
    devices = range(lax.axis_size(axis))
    route = [(i - distance, i) for i in devices if i - distance in devices]
    return lax.ppermute(block, axis, route)


def split_norm(total, gain, shift):
    totals = in_one((jnp.sum(total, axis=1), jnp.sum(total * total, axis=1)), "tp")
    center = totals[0] / D
    spread = totals[1] / D - center * center
    return (total - center[:, None]) * lax.rsqrt(spread + NORM_EPS)[:, None] * gain + shift


def expert_rows(arrived, gate_weight, up_weight, down_weight):
    sources, count, width = arrived.shape
    flat_rows = arrived.reshape(sources * count, width)
    gate = jnp.dot(flat_rows, gate_weight[0], preferred_element_type=jnp.float32)
    up_val = jnp.dot(flat_rows, up_weight[0], preferred_element_type=jnp.float32)
    middle = (jax.nn.silu(gate) * up_val).astype(jnp.bfloat16)
    share_out = jnp.dot(middle, down_weight[0], preferred_element_type=jnp.float32).astype(
        jnp.bfloat16
    )
    groups = lax.axis_size("tp")
    pieces = share_out.reshape(sources, count, groups, width // groups)
    traded = lax.all_to_all(pieces, "tp", split_axis=2, concat_axis=2, tiled=True)
    summed = jnp.sum(traded.astype(jnp.float32), axis=2)
    return lax.all_to_all(
        summed.astype(jnp.bfloat16), "sp", split_axis=0, concat_axis=0, tiled=True
    )


def pack_rows(source_rows, table, expert_count, capacity):
    padded = jnp.concatenate(
        [source_rows, jnp.zeros((1, source_rows.shape[1]), source_rows.dtype)], axis=0
    )
    return padded[table].reshape(expert_count, capacity, source_rows.shape[1])


def local(
    residual,
    queries,
    keys,
    values,
    documents,
    sinks,
    head_gain,
    out_weight,
    norm_gain,
    norm_shift,
    routes,
    route_logits,
    gate_weight,
    up_weight,
    down_weight,
    final_gain,
    final_shift,
):
    tokens = queries.shape[0]
    head_list = sinks.shape[0]
    tails = shifted(
        (
            keys[tokens - WINDOW_SIZE :],
            values[tokens - WINDOW_SIZE :],
            documents[tokens - WINDOW_SIZE :].astype(jnp.bfloat16),
        ),
        "sp",
        1,
    )
    offset = lax.axis_index("sp") * tokens
    shared_key_head = lax.axis_index("tp") * head_list // (QUERY_HEADS // KEY_VALUE_HEADS)
    all_keys = jnp.concatenate([tails[0], keys], axis=0)
    all_values = jnp.concatenate([tails[1], values], axis=0)
    all_docs = jnp.concatenate([tails[2].astype(jnp.int32), documents], axis=0)
    key_head = lax.dynamic_slice_in_dim(all_keys, shared_key_head * HEAD_SIZE, HEAD_SIZE, 1)
    value_head = lax.dynamic_slice_in_dim(all_values, shared_key_head * HEAD_SIZE, HEAD_SIZE, 1)
    query_heads = queries.reshape(tokens, head_list, HEAD_SIZE)
    scores = jnp.einsum(
        "qhd,kd->hqk", query_heads, key_head, preferred_element_type=jnp.float32
    ) * HEAD_SIZE ** (-0.5)
    query_pos = offset + jnp.arange(tokens, dtype=jnp.int32)
    key_pos = offset - WINDOW_SIZE + jnp.arange(tokens + WINDOW_SIZE, dtype=jnp.int32)
    distance = query_pos[:, None] - key_pos[None, :]
    allowed = (
        (distance >= 0)
        & (distance < WINDOW_SIZE)
        & (key_pos[None, :] >= 0)
        & (documents[:, None] == all_docs[None, :])
    )
    scores = jnp.where(allowed[None], scores, -jnp.inf)
    sink_col = sinks[:, None]
    top = jnp.maximum(jnp.max(scores, axis=2), sink_col)
    expd = jnp.exp(scores - top[..., None])
    probs = (expd / (jnp.sum(expd, axis=2) + jnp.exp(sink_col - top))[..., None]).astype(
        jnp.bfloat16
    )
    attended = jnp.einsum("hqk,kd->qhd", probs, value_head, preferred_element_type=jnp.float32)
    attended = attended.astype(jnp.bfloat16).reshape(tokens, head_list * HEAD_SIZE)
    all_heads = lax.all_gather(attended, "tp", axis=1, tiled=True).astype(jnp.float32)
    scaled = (
        all_heads
        * lax.rsqrt(jnp.mean(all_heads * all_heads, axis=1, keepdims=True) + NORM_EPS)
        * head_gain
    ).astype(jnp.bfloat16)
    mix = jnp.dot(scaled, out_weight, preferred_element_type=jnp.float32)
    first = DEEP_ALPHA * residual.astype(jnp.float32) + mix
    hidden = split_norm(first, norm_gain, norm_shift)
    hidden_rows = hidden.astype(jnp.bfloat16)
    expert_count = lax.axis_size("sp")
    capacity = 3 * tokens * TOP // (2 * expert_count)
    flat = routes.reshape(-1)
    onehot = (flat[:, None] == jnp.arange(expert_count, dtype=jnp.int32)[None, :]).astype(jnp.int32)
    rank = jnp.sum(jnp.cumsum(onehot, axis=0) * onehot, axis=1) - 1
    target = flat * capacity + rank
    owner = jnp.arange(tokens * TOP, dtype=jnp.int32) // TOP
    table = jnp.full((expert_count * capacity,), tokens, jnp.int32).at[target].set(owner)
    outgoing = pack_rows(hidden_rows, table, expert_count, capacity)
    joined = lax.all_gather(
        lax.all_to_all(outgoing, "sp", split_axis=0, concat_axis=0, tiled=True),
        "tp",
        axis=2,
        tiled=True,
    )
    returned = expert_rows(joined, gate_weight, up_weight, down_weight)
    picked = (
        returned.reshape(expert_count * capacity, -1)[target]
        .reshape(tokens, TOP, -1)
        .astype(jnp.float32)
    )
    share = jax.nn.softmax(route_logits, axis=-1)
    moe = jnp.sum(share[:, :, None] * picked, axis=1)
    second = DEEP_ALPHA * hidden + moe
    return split_norm(second, final_gain, final_shift).astype(jnp.bfloat16)


def solution(mesh):
    return jax.shard_map(
        local,
        mesh=mesh,
        in_specs=(
            P("sp", "tp"),
            P("sp", "tp"),
            P("sp", None),
            P("sp", None),
            P("sp"),
            P("tp"),
            P(),
            P(None, "tp"),
            P("tp"),
            P("tp"),
            P("sp", None),
            P("sp", None),
            P("sp", None, "tp"),
            P("sp", None, "tp"),
            P("sp", "tp", None),
            P("tp"),
            P("tp"),
        ),
        out_specs=P("sp", "tp"),
        check_vma=False,
    )
```

profile of v0, /device:TPU:1, one launch (start us, length us, event | category | flops | bytes accessed | tf_op | source)
XLA Modules:
  0.0 268.2 jit_solution(7688286295900288744)
XLA Ops:
  6.5 0.9 slice.30
  7.4 3.9 %collective-permute-start.2 = (bf16[128,128]{1,0:T(8,128)(2,1)S(1)}, bf16[128,128]{1,0:T(8,128)(2,1)S(1)}, u32[]{:S(2)}, u32[]{:S(2)}) collective-permute-start(bf16[128,128]{1,0:T(8,128)(2,1)S(1)} %slice.30), channel_id=1, source_target_pairs={{0,16},{16,32},{32,48},{48,64},{64,80},{80,96},{96,112},{112,128},... | collective-permute-start | bytes 98312 | tf_op jit(solution)/shard_map/ppermute | solution.py:39
  11.4 0.7 convert.5
  12.0 3.1 %collective-permute-start.1 = (bf16[128]{0:T(256)(128)(2,1)S(1)}, bf16[128]{0:T(256)(128)(2,1)S(1)}, u32[]{:S(2)}, u32[]{:S(2)}) collective-permute-start(bf16[128]{0:T(256)(128)(2,1)S(1)} %slice.29), channel_id=1, source_target_pairs={{0,16},{16,32},{32,48},{48,64},{64,80},{80,96},{96,112},{112,128},... | collective-permute-start | bytes 776 | tf_op jit(solution)/shard_map/ppermute | solution.py:39
  15.2 0.8 slice.28
  15.9 2.8 %collective-permute-start = (bf16[128,128]{1,0:T(8,128)(2,1)S(1)}, bf16[128,128]{1,0:T(8,128)(2,1)S(1)}, u32[]{:S(2)}, u32[]{:S(2)}) collective-permute-start(bf16[128,128]{1,0:T(8,128)(2,1)S(1)} %slice.28), channel_id=1, source_target_pairs={{0,16},{16,32},{32,48},{48,64},{64,80},{80,96},{96,112},{112,128},... | collective-permute-start | bytes 98312 | tf_op jit(solution)/shard_map/ppermute | solution.py:39
  18.8 0.8 copy.39
  19.6 0.1 eq.52
  19.8 0.1 eq.48
  19.9 0.7 broadcast_multiply_fusion
  20.6 1.2 reduce-window.6
  21.8 0.2 slice_reduce_fusion
  22.0 0.1 fusion.39
  22.2 0.1 copy.38
  22.3 0.1 mul.144
  22.5 2.4 scatter_custom_fusion
  25.6 0.7 pad_add_fusion
  26.3 1.2 fusion.55
  27.5 0.0 copy-start.8
  27.5 0.1 fusion.28
  27.7 0.3 fusion.14
  28.0 20.4 %all-gather = bf16[256,1,1024]{0,2,1:T(8,128)(2,1)S(1)} all-gather(bf16[256,1,64]{0,2,1:T(8,128)(2,1)S(1)} %fusion.14), channel_id=2, replica_groups=mesh['sp'=32,'tp'=16] {'tp'}, dimensions={2}, use_global_device_ids=true | all-gather | bytes 557056 | tf_op jit(solution)/shard_map/all_gather | solution.py:133
  48.3 0.2 fusion.15
  48.6 0.7 fusion.54
  49.2 0.6 broadcast_in_dim.13
  49.9 4.5 %all-to-all-start = ((f32[16,1,512]{2,1,0:T(1,128)}), f32[16,1,512]{2,1,0:T(1,128)S(1)}, u32[]{:S(2)}, u32[]{:S(2)}) async-start(f32[16,1,512]{2,1,0:T(1,128)} %broadcast_in_dim.13), calls=%async_computation | async-start | bytes 65536 | tf_op jit(solution)/shard_map/all_to_all | solution.py:18
  54.4 0.0 all-gather.3.cloned.1.call-start
  54.4 7.3 %all-to-all-done = f32[16,1,512]{2,1,0:T(1,128)S(1)} async-done(((f32[16,1,512]{2,1,0:T(1,128)}), f32[16,1,512]{2,1,0:T(1,128)S(1)}, u32[]{:S(2)}, u32[]{:S(2)}) %all-to-all-start) | async-done | bytes 32800 | tf_op jit(solution)/shard_map/all_to_all | solution.py:18
  61.8 0.1 fusion.31
  62.0 1.9 gather_fusion
  63.9 23.3 %all_to_all.27 = bf16[32,24,128]{2,1,0:T(8,128)(2,1)} all-to-all(bf16[32,24,128]{2,1,0:T(8,128)(2,1)S(1)} %bitcast.72), channel_id=1, replica_groups=mesh['sp'=32,'tp'=16] {'sp'}, dimensions={0} | all-to-all | bytes 393216 | tf_op jit(solution)/shard_map/all_to_all | solution.py:153
  87.2 0.0 all-gather.3.cloned.1.call-update
  87.2 39.9 %all-gather.3.cloned.1.call-done = bf16[32,24,2048]{2,1,0:T(8,128)(2,1)} async-done(((bf16[32,24,128]{2,1,0:T(8,128)(2,1)}), bf16[32,24,2048]{2,1,0:T(8,128)(2,1)}) %all-gather.3.cloned.1.call-update) | async-done | bytes 3145744 | tf_op jit(solution)/shard_map/all_gather | solution.py:152
  127.1 5.3 %fusion.4 = f32[768,384]{1,0:T(8,128)} fusion(bf16[768,2048]{1,0:T(8,128)(2,1)} %bitcast.77, bf16[1,2048,384]{2,1,0:T(8,128)(2,1)} %param.29), kind=kOutput, calls=%fused_computation.8 | convolution fusion | flops 1207959552 | bytes 5898240 | tf_op jit(solution)/shard_map/dot_general | solution.py:52
  132.4 7.4 %fusion = bf16[96,8,16,128]{3,1,2,0:T(8,128)(2,1)} fusion(bf16[1,384,2048]{2,1,0:T(8,128)(2,1)S(1)} %copy-done, bf16[768,2048]{1,0:T(8,128)(2,1)} %bitcast.78, bf16[1,2048,384]{2,1,0:T(8,128)(2,1)S(1)} %copy-done.7, f32[768,384]{1,0:T(8,128)} %fusion.4), kind=kOutput, calls=%fused_computation.4 | convolution fusion | flops 2419261440 | bytes 10616832 | tf_op jit(solution)/shard_map/dot_general | solution.py:55
  139.7 2.9 %copy.51 = bf16[96,8,16,128]{3,2,1,0:T(8,128)(2,1)S(1)} copy(bf16[96,8,16,128]{3,1,2,0:T(8,128)(2,1)} %fusion) | data formatting | bytes 6291456
  142.6 2.5 copy.42
  145.2 4.6 %all-to-all-start.2 = ((bf16[32,24,16,128]{3,1,0,2:T(8,128)(2,1)}), bf16[32,24,16,128]{3,1,0,2:T(8,128)(2,1)}, u32[]{:S(2)}, u32[]{:S(2)}) async-start(bf16[32,24,16,128]{3,1,0,2:T(8,128)(2,1)} %copy.42), calls=%async_computation.2 | async-start | bytes 6291456 | tf_op jit(solution)/shard_map/all_to_all | solution.py:60
  149.8 71.1 %all-to-all-done.2 = bf16[32,24,16,128]{3,1,0,2:T(8,128)(2,1)} async-done(((bf16[32,24,16,128]{3,1,0,2:T(8,128)(2,1)}), bf16[32,24,16,128]{3,1,0,2:T(8,128)(2,1)}, u32[]{:S(2)}, u32[]{:S(2)}) %all-to-all-start.2) | async-done | bytes 3145760 | tf_op jit(solution)/shard_map/all_to_all | solution.py:60
  220.9 3.1 %reduce_sum.118 = bf16[32,24,128]{2,1,0:T(8,128)(2,1)} reduce(bf16[32,24,16,128]{3,1,0,2:T(8,128)(2,1)} %all-to-all-done.2, bf16[]{:T(256)} %constant.87.clone.1), dimensions={2}, to_apply=%region_12.13 | reduce | flops 1474560 | bytes 3342338 | tf_op jit(solution)/shard_map/reduce_sum | solution.py:61
  223.9 9.7 %all-to-all-start.3 = ((bf16[32,24,128]{2,1,0:T(8,128)(2,1)}), bf16[32,24,128]{2,1,0:T(8,128)(2,1)S(1)}, u32[]{:S(2)}, u32[]{:S(2)}) async-start(bf16[32,24,128]{2,1,0:T(8,128)(2,1)} %reduce_sum.118), calls=%async_computation.3 | async-start | bytes 393216 | tf_op jit(solution)/shard_map/all_to_all | solution.py:62
  233.7 0.1 copy.37
  233.9 9.7 %all-to-all-done.3 = bf16[32,24,128]{2,1,0:T(8,128)(2,1)S(1)} async-done(((bf16[32,24,128]{2,1,0:T(8,128)(2,1)}), bf16[32,24,128]{2,1,0:T(8,128)(2,1)S(1)}, u32[]{:S(2)}, u32[]{:S(2)}) %all-to-all-start.3) | async-done | bytes 196640 | tf_op jit(solution)/shard_map/all_to_all | solution.py:62
  243.6 1.3 gather_fusion.1
  244.9 0.4 fusion.29
  245.3 0.3 fusion.53
  245.6 14.9 %all_to_all.28 = f32[16,1,512]{2,1,0:T(1,128)S(1)} all-to-all(f32[16,1,512]{2,1,0:T(1,128)S(1)} %broadcast_in_dim.16), channel_id=1, replica_groups=mesh['sp'=32,'tp'=16] {'tp'}, dimensions={0} | all-to-all | bytes 65536 | tf_op jit(solution)/shard_map/all_to_all | solution.py:18
  260.6 0.8 add_convert_fusion
  (52 shorter events, 0.4 us)
Async XLA Ops:
  6.5 125.8 %copy-start = (bf16[1,384,2048]{2,1,0:T(8,128)(2,1)S(1)}, bf16[1,384,2048]{2,1,0:T(8,128)(2,1)}, u32[]{:S(2)}) copy-start(bf16[1,384,2048]{2,1,0:T(8,128)(2,1)} %param.31) | copy-start | bytes 4718596
  6.5 21.1 %copy-start.2 = (bf16[256,128]{1,0:T(8,128)(2,1)S(1)}, bf16[256,128]{1,0:T(8,128)(2,1)}, u32[]{:S(2)}) copy-start(bf16[256,128]{1,0:T(8,128)(2,1)} %param.20) | copy-start | bytes 196612
  7.4 18.9 %collective-permute-start.2 = (bf16[128,128]{1,0:T(8,128)(2,1)S(1)}, bf16[128,128]{1,0:T(8,128)(2,1)S(1)}, u32[]{:S(2)}, u32[]{:S(2)}) collective-permute-start(bf16[128,128]{1,0:T(8,128)(2,1)S(1)} %slice.30), channel_id=1, source_target_pairs={{0,16},{16,32},{32,48},{48,64},{64,80},{80,96},{96,112},{112,128},... | collective-permute-start | bytes 98312 | tf_op jit(solution)/shard_map/ppermute | solution.py:39
  12.0 13.5 %collective-permute-start.1 = (bf16[128]{0:T(256)(128)(2,1)S(1)}, bf16[128]{0:T(256)(128)(2,1)S(1)}, u32[]{:S(2)}, u32[]{:S(2)}) collective-permute-start(bf16[128]{0:T(256)(128)(2,1)S(1)} %slice.29), channel_id=1, source_target_pairs={{0,16},{16,32},{32,48},{48,64},{64,80},{80,96},{96,112},{112,128},... | collective-permute-start | bytes 776 | tf_op jit(solution)/shard_map/ppermute | solution.py:39
  15.9 11.7 %collective-permute-start = (bf16[128,128]{1,0:T(8,128)(2,1)S(1)}, bf16[128,128]{1,0:T(8,128)(2,1)S(1)}, u32[]{:S(2)}, u32[]{:S(2)}) collective-permute-start(bf16[128,128]{1,0:T(8,128)(2,1)S(1)} %slice.28), channel_id=1, source_target_pairs={{0,16},{16,32},{32,48},{48,64},{64,80},{80,96},{96,112},{112,128},... | collective-permute-start | bytes 98312 | tf_op jit(solution)/shard_map/ppermute | solution.py:39
  27.5 21.0 %copy-start.8 = (bf16[1024,128]{1,0:T(8,128)(2,1)S(1)}, bf16[1024,128]{1,0:T(8,128)(2,1)}, u32[]{:S(2)}) copy-start(bf16[1024,128]{1,0:T(8,128)(2,1)} %param.24) | copy-start | bytes 786436
  27.5 21.0 %copy-start.9 = (bf16[256,128]{1,0:T(8,128)(2,1)S(1)}, bf16[256,128]{1,0:T(8,128)(2,1)}, u32[]{:S(2)}) copy-start(bf16[256,128]{1,0:T(8,128)(2,1)} %param.17) | copy-start | bytes 196612
  27.5 21.0 %copy-start.10 = (f32[1024]{0:T(1024)S(1)}, f32[1024]{0:T(1024)}, u32[]{:S(2)}) copy-start(f32[1024]{0:T(1024)} %param.23) | copy-start | bytes 12292
  27.9 33.9 %copy-start.3 = (f32[128]{0:T(128)S(1)}, f32[128]{0:T(128)}, u32[]{:S(2)}) copy-start(f32[128]{0:T(128)} %param.26) | copy-start | bytes 1540
  28.0 33.8 %copy-start.4 = (f32[128]{0:T(128)S(1)}, f32[128]{0:T(128)}, u32[]{:S(2)}) copy-start(f32[128]{0:T(128)} %param.25) | copy-start | bytes 1540
  49.9 11.9 %all-to-all-start = ((f32[16,1,512]{2,1,0:T(1,128)}), f32[16,1,512]{2,1,0:T(1,128)S(1)}, u32[]{:S(2)}, u32[]{:S(2)}) async-start(f32[16,1,512]{2,1,0:T(1,128)} %broadcast_in_dim.13), calls=%async_computation | async-start | bytes 65536 | tf_op jit(solution)/shard_map/all_to_all | solution.py:18
  54.4 72.7 %all-gather.3.cloned.1.call-start = ((), (), s32[]{:S(2)}) async-start(), calls=%async_computation.5 | async-start | bytes 3342336 | tf_op jit(solution)/shard_map/all_gather | solution.py:152
  127.1 5.3 %copy-start.7 = (bf16[1,2048,384]{2,1,0:T(8,128)(2,1)S(1)}, bf16[1,2048,384]{2,1,0:T(8,128)(2,1)}, u32[]{:S(2)}) copy-start(bf16[1,2048,384]{2,1,0:T(8,128)(2,1)} %param.30) | copy-start | bytes 4718596
  145.2 4.6 %copy-start.1 = (f32[256,2]{0,1:T(2,128)S(1)}, f32[256,2]{0,1:T(2,128)}, u32[]{:S(2)}) copy-start(f32[256,2]{0,1:T(2,128)} %param.28) | copy-start | bytes 6148
  145.2 75.7 %all-to-all-start.2 = ((bf16[32,24,16,128]{3,1,0,2:T(8,128)(2,1)}), bf16[32,24,16,128]{3,1,0,2:T(8,128)(2,1)}, u32[]{:S(2)}, u32[]{:S(2)}) async-start(bf16[32,24,16,128]{3,1,0,2:T(8,128)(2,1)} %copy.42), calls=%async_computation.2 | async-start | bytes 6291456 | tf_op jit(solution)/shard_map/all_to_all | solution.py:60
  223.9 36.6 %copy-start.5 = (f32[128]{0:T(128)S(1)}, f32[128]{0:T(128)}, u32[]{:S(2)}) copy-start(f32[128]{0:T(128)} %param.33) | copy-start | bytes 1540
  223.9 36.6 %copy-start.6 = (f32[128]{0:T(128)S(1)}, f32[128]{0:T(128)}, u32[]{:S(2)}) copy-start(f32[128]{0:T(128)} %param.32) | copy-start | bytes 1540
  223.9 19.6 %all-to-all-start.3 = ((bf16[32,24,128]{2,1,0:T(8,128)(2,1)}), bf16[32,24,128]{2,1,0:T(8,128)(2,1)S(1)}, u32[]{:S(2)}, u32[]{:S(2)}) async-start(bf16[32,24,128]{2,1,0:T(8,128)(2,1)} %reduce_sum.118), calls=%async_computation.3 | async-start | bytes 393216 | tf_op jit(solution)/shard_map/all_to_all | solution.py:62
Sparse Core Ops, SparseCore 0:
  87.3 39.7 all-gather.2
where the time goes:
time: 269 us; the launch traced here: 268 us
  waiting for transfers between devices  128 us (48%)
  blocking collectives  58.5 us (22%)
  starting transfers between devices  28.7 us (11%)
  local copies, waits for them, and re-layouts  15.2 us (6%)
  matrix products  14.8 us (6%)
  between operations  14.4 us (5%)
  other arithmetic  8.54 us (3%)
    all_to_all x1, waiting for transfers between devices, expert_rows(): lax.all_to_all(pieces, 'tp', split_axis=2, concat_axis=2, tiled=True)  71.1 us
    all_gather x1, waiting for transfers between devices, local(): lax.all_gather(lax.all_to_all(outgoing, 'sp', split_axis=0, concat_axis=0...  39.9 us
    all_to_all x1, blocking collectives, local(): lax.all_to_all(outgoing, 'sp', split_axis=0, concat_axis=0, tiled=True)  23.3 us
    all_gather x1, blocking collectives, local(): lax.all_gather(attended, 'tp', axis=1, tiled=True).astype(jnp.float32)  20.4 us
    all_to_all x1, blocking collectives, sent_to_all(): lax.all_to_all(jnp.broadcast_to(value[None], (length, *value.shape)), axi...  14.9 us
    ppermute x3, starting transfers between devices, shifted(): return lax.ppermute(block, axis, route)  9.84 us
    all_to_all x1, starting transfers between devices, expert_rows(): lax.all_to_all(summed.astype(jnp.bfloat16), 'sp', split_axis=0, concat_ax...  9.73 us
    all_to_all x1, waiting for transfers between devices, expert_rows(): lax.all_to_all(summed.astype(jnp.bfloat16), 'sp', split_axis=0, concat_ax...  9.68 us
  transfers between devices with their start and end apart: 7, of which 4 were waited for; matrix products, arithmetic and copies ran while one was open for 4% of the time, Pallas kernels for 0%

commit v1 on v0

--- a/solution.py
+++ b/solution.py
@@ -149,12 +149,9 @@
     owner = jnp.arange(tokens * TOP, dtype=jnp.int32) // TOP
     table = jnp.full((expert_count * capacity,), tokens, jnp.int32).at[target].set(owner)
     outgoing = pack_rows(hidden_rows, table, expert_count, capacity)
-    joined = lax.all_gather(
-        lax.all_to_all(outgoing, "sp", split_axis=0, concat_axis=0, tiled=True),
-        "tp",
-        axis=2,
-        tiled=True,
-    )
+    part = lax.all_to_all(outgoing, "sp", split_axis=0, concat_axis=0, tiled=True)
+    outgoing_2 = jnp.stack([part] * lax.axis_size("tp"))
+    joined = jnp.concatenate(lax.all_to_all(outgoing_2, "tp", 0, 0), axis=2)
     returned = expert_rows(joined, gate_weight, up_weight, down_weight)
     picked = (
         returned.reshape(expert_count * capacity, -1)[target]

time: 269 us -> 290 us (1.078)
  blocking collectives: 58.5 us -> 136 us
  waiting for transfers between devices: 128 us -> 86.9 us
  between operations: 14.4 us -> 1.04 us
  local copies, waits for them, and re-layouts: 15.2 us -> 21.1 us
  starting transfers between devices: 28.7 us -> 22.8 us
    all_to_all x0 -> x1, blocking collectives: none -> 77.8 us  [local(): joined = jnp.concatenate(lax.all_to_all(outgoing_2, 'tp', 0, 0), axis=2)]
    all_gather x1 -> x0, waiting for transfers between devices: 39.9 us -> none  [local(): lax.all_gather(lax.all_to_all(outgoing, 'sp', split_axis=0, concat_axis=0...]
    all_to_all x1, starting transfers between devices: 9.73 us -> 4 us  [expert_rows(): lax.all_to_all(summed.astype(jnp.bfloat16), 'sp', split_axis=0, concat_ax...]
    reshape x0 -> x1, local copies, waits for them, and re-layouts: none -> 3.64 us  [local(): joined = jnp.concatenate(lax.all_to_all(outgoing_2, 'tp', 0, 0), axis=2)]
  transfers between devices with their start and end apart: 7 -> 6, of which waited for: 4 -> 3; matrix products, arithmetic and copies ran while one was open for 4% -> 3% of each run, Pallas kernels for 0% -> 0%
where the time goes in v1:
time: 290 us; the launch traced here: 289 us
  blocking collectives  136 us (47%)
  waiting for transfers between devices  86.9 us (30%)
  starting transfers between devices  22.8 us (8%)
  local copies, waits for them, and re-layouts  21.1 us (7%)
  matrix products  12.3 us (4%)
  other arithmetic  8.54 us (3%)
    all_to_all x1, blocking collectives, local(): joined = jnp.concatenate(lax.all_to_all(outgoing_2, 'tp', 0, 0), axis=2)  77.8 us
    all_to_all x1, waiting for transfers between devices, expert_rows(): lax.all_to_all(pieces, 'tp', split_axis=2, concat_axis=2, tiled=True)  69.7 us
    all_to_all x1, blocking collectives, local(): lax.all_to_all(outgoing, 'sp', split_axis=0, concat_axis=0, tiled=True)  23.2 us
    all_gather x1, blocking collectives, local(): lax.all_gather(attended, 'tp', axis=1, tiled=True).astype(jnp.float32)  20.4 us
    all_to_all x1, blocking collectives, sent_to_all(): lax.all_to_all(jnp.broadcast_to(value[None], (length, *value.shape)), axi...  15 us
    ppermute x3, starting transfers between devices, shifted(): return lax.ppermute(block, axis, route)  9.84 us
    all_to_all x1, waiting for transfers between devices, expert_rows(): lax.all_to_all(summed.astype(jnp.bfloat16), 'sp', split_axis=0, concat_ax...  9.78 us
    all_to_all x1, waiting for transfers between devices, sent_to_all(): lax.all_to_all(jnp.broadcast_to(value[None], (length, *value.shape)), axi...  7.38 us
  transfers between devices with their start and end apart: 6, of which 3 were waited for; matrix products, arithmetic and copies ran while one was open for 3% of the time, Pallas kernels for 0%

profile of v1, /device:TPU:1, one launch (start us, length us, event | category | flops | bytes accessed | tf_op | source)
XLA Modules:
  0.0 289.1 jit_solution(8624790257206008477)
XLA Ops:
  0.0 0.9 slice.30
  0.9 3.9 %collective-permute-start.2 = (bf16[128,128]{1,0:T(8,128)(2,1)S(1)}, bf16[128,128]{1,0:T(8,128)(2,1)S(1)}, u32[]{:S(2)}, u32[]{:S(2)}) collective-permute-start(bf16[128,128]{1,0:T(8,128)(2,1)S(1)} %slice.30), channel_id=1, source_target_pairs={{0,16},{16,32},{32,48},{48,64},{64,80},{80,96},{96,112},{112,128},... | collective-permute-start | bytes 98312 | tf_op jit(solution)/shard_map/ppermute | solution.py:39
  4.8 0.7 convert.5
  5.5 3.1 %collective-permute-start.1 = (bf16[128]{0:T(256)(128)(2,1)S(1)}, bf16[128]{0:T(256)(128)(2,1)S(1)}, u32[]{:S(2)}, u32[]{:S(2)}) collective-permute-start(bf16[128]{0:T(256)(128)(2,1)S(1)} %slice.29), channel_id=1, source_target_pairs={{0,16},{16,32},{32,48},{48,64},{64,80},{80,96},{96,112},{112,128},... | collective-permute-start | bytes 776 | tf_op jit(solution)/shard_map/ppermute | solution.py:39
  8.6 0.8 slice.28
  9.4 2.8 collective-permute-start
  12.3 0.8 copy.41
  13.1 0.1 eq.52
  13.2 0.1 eq.48
  13.4 0.7 broadcast_multiply_fusion
  14.1 1.2 reduce-window.6
  15.2 0.2 slice_reduce_fusion
  15.5 0.1 fusion.49
  15.6 0.1 copy.40
  15.8 0.1 mul.144
  15.9 2.4 scatter_custom_fusion
  19.1 0.7 pad_add_fusion
  19.8 1.2 fusion.65
  21.0 0.1 fusion.38
  21.1 0.3 fusion.22
  21.4 20.4 %all-gather = bf16[256,1,1024]{0,2,1:T(8,128)(2,1)S(1)} all-gather(bf16[256,1,64]{0,2,1:T(8,128)(2,1)S(1)} %fusion.22), channel_id=2, replica_groups=mesh['sp'=32,'tp'=16] {'tp'}, dimensions={2}, use_global_device_ids=true | all-gather | bytes 557056 | tf_op jit(solution)/shard_map/all_gather | solution.py:133
  41.8 0.2 fusion.23
  42.0 0.7 fusion.64
  42.7 0.6 broadcast_in_dim.13
  43.3 4.5 %all-to-all-start = ((f32[16,1,512]{2,1,0:T(1,128)}), f32[16,1,512]{2,1,0:T(1,128)S(1)}, u32[]{:S(2)}, u32[]{:S(2)}) async-start(f32[16,1,512]{2,1,0:T(1,128)} %broadcast_in_dim.13), calls=%async_computation | async-start | bytes 65536 | tf_op jit(solution)/shard_map/all_to_all | solution.py:18
  47.8 7.4 %all-to-all-done = f32[16,1,512]{2,1,0:T(1,128)S(1)} async-done(((f32[16,1,512]{2,1,0:T(1,128)}), f32[16,1,512]{2,1,0:T(1,128)S(1)}, u32[]{:S(2)}, u32[]{:S(2)}) %all-to-all-start) | async-done | bytes 32800 | tf_op jit(solution)/shard_map/all_to_all | solution.py:18
  55.3 0.1 fusion.41
  55.4 1.9 gather_fusion
  57.3 23.2 %all_to_all.32 = bf16[32,24,128]{2,1,0:T(8,128)(2,1)S(1)} all-to-all(bf16[32,24,128]{2,1,0:T(8,128)(2,1)S(1)} %bitcast.86), channel_id=1, replica_groups=mesh['sp'=32,'tp'=16] {'sp'}, dimensions={0} | all-to-all | bytes 393216 | tf_op jit(solution)/shard_map/all_to_all | solution.py:152
  80.5 0.6 stack.2
  81.1 77.8 %all_to_all.33 = bf16[16,32,24,128]{3,2,1,0:T(8,128)(2,1)S(1)} all-to-all(bf16[16,32,24,128]{3,2,1,0:T(8,128)(2,1)S(1)} %stack.2), channel_id=1, replica_groups=mesh['sp'=32,'tp'=16] {'tp'}, dimensions={0} | all-to-all | bytes 6291456 | tf_op jit(solution)/shard_map/all_to_all | solution.py:154
  158.9 3.6 %copy.44 = bf16[32,24,16,128]{3,2,1,0:T(8,128)(2,1)S(1)} copy(bf16[32,24,16,128]{3,1,0,2:T(8,128)(2,1)S(1)} %bitcast.81) | data formatting | bytes 6291456 | tf_op jit(solution)/shard_map/reshape | solution.py:154
  162.6 1.7 copy-done.1
  164.2 2.8 fusion.2
  167.1 7.4 %fusion.6 = bf16[96,8,16,128]{3,1,2,0:T(8,128)(2,1)} fusion(bf16[1,384,2048]{2,1,0:T(8,128)(2,1)S(1)} %copy-done, bf16[1,2048,384]{2,1,0:T(8,128)(2,1)S(1)} %copy-done.9, bf16[96,8,16,128]{3,2,1,0:T(8,128)(2,1)} %bitcast.85, f32[768,384]{1,0:T(8,128)} %fusion.2), kind=kOutput, calls=%fused_computation.10 | convolution fusion | flops 2419261440 | bytes 10616832 | tf_op jit(solution)/shard_map/dot_general | solution.py:55
  174.4 2.9 %copy.55 = bf16[96,8,16,128]{3,2,1,0:T(8,128)(2,1)S(1)} copy(bf16[96,8,16,128]{3,1,2,0:T(8,128)(2,1)} %fusion.6) | data formatting | bytes 6291456
  177.3 2.5 copy.45
  179.9 4.5 %all-to-all-start.3 = ((bf16[32,24,16,128]{3,1,0,2:T(8,128)(2,1)}), bf16[32,24,16,128]{3,1,0,2:T(8,128)(2,1)}, u32[]{:S(2)}, u32[]{:S(2)}) async-start(bf16[32,24,16,128]{3,1,0,2:T(8,128)(2,1)} %copy.45), calls=%async_computation.3 | async-start | bytes 6291456 | tf_op jit(solution)/shard_map/all_to_all | solution.py:60
  184.4 69.7 %all-to-all-done.3 = bf16[32,24,16,128]{3,1,0,2:T(8,128)(2,1)} async-done(((bf16[32,24,16,128]{3,1,0,2:T(8,128)(2,1)}), bf16[32,24,16,128]{3,1,0,2:T(8,128)(2,1)}, u32[]{:S(2)}, u32[]{:S(2)}) %all-to-all-start.3) | async-done | bytes 3145760 | tf_op jit(solution)/shard_map/all_to_all | solution.py:60
  254.1 3.1 %reduce_sum.118 = bf16[32,24,128]{2,1,0:T(8,128)(2,1)} reduce(bf16[32,24,16,128]{3,1,0,2:T(8,128)(2,1)} %all-to-all-done.3, bf16[]{:T(256)} %constant.87.clone.1), dimensions={2}, to_apply=%region_12.13 | reduce | flops 1474560 | bytes 3342338 | tf_op jit(solution)/shard_map/reduce_sum | solution.py:61
  257.2 4.0 %all-to-all-start.4 = ((bf16[32,24,128]{2,1,0:T(8,128)(2,1)}), bf16[32,24,128]{2,1,0:T(8,128)(2,1)S(1)}, u32[]{:S(2)}, u32[]{:S(2)}) async-start(bf16[32,24,128]{2,1,0:T(8,128)(2,1)} %reduce_sum.118), calls=%async_computation.4 | async-start | bytes 393216 | tf_op jit(solution)/shard_map/all_to_all | solution.py:62
  261.2 0.1 copy.39
  261.4 9.8 %all-to-all-done.4 = bf16[32,24,128]{2,1,0:T(8,128)(2,1)S(1)} async-done(((bf16[32,24,128]{2,1,0:T(8,128)(2,1)}), bf16[32,24,128]{2,1,0:T(8,128)(2,1)S(1)}, u32[]{:S(2)}, u32[]{:S(2)}) %all-to-all-start.4) | async-done | bytes 196640 | tf_op jit(solution)/shard_map/all_to_all | solution.py:62
  271.2 1.3 gather_fusion.1
  272.5 0.4 fusion.39
  272.9 0.3 fusion.63
  273.2 15.0 %all_to_all.34 = f32[16,1,512]{2,1,0:T(1,128)S(1)} all-to-all(f32[16,1,512]{2,1,0:T(1,128)S(1)} %broadcast_in_dim.16), channel_id=1, replica_groups=mesh['sp'=32,'tp'=16] {'tp'}, dimensions={0} | all-to-all | bytes 65536 | tf_op jit(solution)/shard_map/all_to_all | solution.py:18
  288.3 0.8 add_convert_fusion
  (56 shorter events, 0.4 us)
Async XLA Ops:
  0.0 167.1 %copy-start = (bf16[1,384,2048]{2,1,0:T(8,128)(2,1)S(1)}, bf16[1,384,2048]{2,1,0:T(8,128)(2,1)}, u32[]{:S(2)}) copy-start(bf16[1,384,2048]{2,1,0:T(8,128)(2,1)} %param.31) | copy-start | bytes 4718596
  0.0 21.1 %copy-start.3 = (bf16[256,128]{1,0:T(8,128)(2,1)S(1)}, bf16[256,128]{1,0:T(8,128)(2,1)}, u32[]{:S(2)}) copy-start(bf16[256,128]{1,0:T(8,128)(2,1)} %param.20) | copy-start | bytes 196612
  0.9 18.9 %collective-permute-start.2 = (bf16[128,128]{1,0:T(8,128)(2,1)S(1)}, bf16[128,128]{1,0:T(8,128)(2,1)S(1)}, u32[]{:S(2)}, u32[]{:S(2)}) collective-permute-start(bf16[128,128]{1,0:T(8,128)(2,1)S(1)} %slice.30), channel_id=1, source_target_pairs={{0,16},{16,32},{32,48},{48,64},{64,80},{80,96},{96,112},{112,128},... | collective-permute-start | bytes 98312 | tf_op jit(solution)/shard_map/ppermute | solution.py:39
  5.5 13.5 %collective-permute-start.1 = (bf16[128]{0:T(256)(128)(2,1)S(1)}, bf16[128]{0:T(256)(128)(2,1)S(1)}, u32[]{:S(2)}, u32[]{:S(2)}) collective-permute-start(bf16[128]{0:T(256)(128)(2,1)S(1)} %slice.29), channel_id=1, source_target_pairs={{0,16},{16,32},{32,48},{48,64},{64,80},{80,96},{96,112},{112,128},... | collective-permute-start | bytes 776 | tf_op jit(solution)/shard_map/ppermute | solution.py:39
  9.4 11.7 %collective-permute-start = (bf16[128,128]{1,0:T(8,128)(2,1)S(1)}, bf16[128,128]{1,0:T(8,128)(2,1)S(1)}, u32[]{:S(2)}, u32[]{:S(2)}) collective-permute-start(bf16[128,128]{1,0:T(8,128)(2,1)S(1)} %slice.28), channel_id=1, source_target_pairs={{0,16},{16,32},{32,48},{48,64},{64,80},{80,96},{96,112},{112,128},... | collective-permute-start | bytes 98312 | tf_op jit(solution)/shard_map/ppermute | solution.py:39
  21.0 21.0 %copy-start.10 = (bf16[1024,128]{1,0:T(8,128)(2,1)S(1)}, bf16[1024,128]{1,0:T(8,128)(2,1)}, u32[]{:S(2)}) copy-start(bf16[1024,128]{1,0:T(8,128)(2,1)} %param.24) | copy-start | bytes 786436
  21.0 21.0 %copy-start.11 = (bf16[256,128]{1,0:T(8,128)(2,1)S(1)}, bf16[256,128]{1,0:T(8,128)(2,1)}, u32[]{:S(2)}) copy-start(bf16[256,128]{1,0:T(8,128)(2,1)} %param.17) | copy-start | bytes 196612
  21.0 21.0 %copy-start.12 = (f32[1024]{0:T(1024)S(1)}, f32[1024]{0:T(1024)}, u32[]{:S(2)}) copy-start(f32[1024]{0:T(1024)} %param.23) | copy-start | bytes 12292
  21.4 33.8 %copy-start.4 = (f32[128]{0:T(128)S(1)}, f32[128]{0:T(128)}, u32[]{:S(2)}) copy-start(f32[128]{0:T(128)} %param.26) | copy-start | bytes 1540
  21.4 33.8 %copy-start.5 = (f32[128]{0:T(128)S(1)}, f32[128]{0:T(128)}, u32[]{:S(2)}) copy-start(f32[128]{0:T(128)} %param.25) | copy-start | bytes 1540
  43.3 11.9 %all-to-all-start = ((f32[16,1,512]{2,1,0:T(1,128)}), f32[16,1,512]{2,1,0:T(1,128)S(1)}, u32[]{:S(2)}, u32[]{:S(2)}) async-start(f32[16,1,512]{2,1,0:T(1,128)} %broadcast_in_dim.13), calls=%async_computation | async-start | bytes 65536 | tf_op jit(solution)/shard_map/all_to_all | solution.py:18
  158.9 5.3 %copy-start.8 = (bf16[1,2048,384]{2,1,0:T(8,128)(2,1)S(1)}, bf16[1,2048,384]{2,1,0:T(8,128)(2,1)}, u32[]{:S(2)}) copy-start(bf16[1,2048,384]{2,1,0:T(8,128)(2,1)} %param.29) | copy-start | bytes 4718596
  162.6 1.7 copy-start.1
  164.2 2.8 copy-start.9
  179.9 4.5 %copy-start.2 = (f32[256,2]{0,1:T(2,128)S(1)}, f32[256,2]{0,1:T(2,128)}, u32[]{:S(2)}) copy-start(f32[256,2]{0,1:T(2,128)} %param.28) | copy-start | bytes 6148
  179.9 74.3 %all-to-all-start.3 = ((bf16[32,24,16,128]{3,1,0,2:T(8,128)(2,1)}), bf16[32,24,16,128]{3,1,0,2:T(8,128)(2,1)}, u32[]{:S(2)}, u32[]{:S(2)}) async-start(bf16[32,24,16,128]{3,1,0,2:T(8,128)(2,1)} %copy.45), calls=%async_computation.3 | async-start | bytes 6291456 | tf_op jit(solution)/shard_map/all_to_all | solution.py:60
  257.2 31.1 %copy-start.6 = (f32[128]{0:T(128)S(1)}, f32[128]{0:T(128)}, u32[]{:S(2)}) copy-start(f32[128]{0:T(128)} %param.33) | copy-start | bytes 1540
  257.2 31.1 %copy-start.7 = (f32[128]{0:T(128)S(1)}, f32[128]{0:T(128)}, u32[]{:S(2)}) copy-start(f32[128]{0:T(128)} %param.32) | copy-start | bytes 1540
  257.2 14.0 %all-to-all-start.4 = ((bf16[32,24,128]{2,1,0:T(8,128)(2,1)}), bf16[32,24,128]{2,1,0:T(8,128)(2,1)S(1)}, u32[]{:S(2)}, u32[]{:S(2)}) async-start(bf16[32,24,128]{2,1,0:T(8,128)(2,1)} %reduce_sum.118), calls=%async_computation.4 | async-start | bytes 393216 | tf_op jit(solution)/shard_map/all_to_all | solution.py:62
